TPU v7x, 32 devices: a whole 2x2x4 slice. The times are simulated.
32 devices in a mesh: sp: 16 (over z, y, x), tp: 2 (over core).
Axes of the slice: x: 2, y: 2, z: 4, core: 2. Of those that a mesh axis runs over, the one named last changes fastest.
Arguments:
- resid: bfloat16 [4096, 2048], P(('sp', 'tp')), may hold values from -6 to 6
- queries: bfloat16 [4096, 2048], P('sp', 'tp'), may hold values from -6 to 6
- keys: bfloat16 [4096, 1024], P('sp', 'tp'), may hold values from -6 to 6
- values: bfloat16 [4096, 1024], P('sp', 'tp'), may hold values from -6 to 6
- log_gates: float32 [16, 4096], P('tp'), as said below
- documents: int32 [4096], P('sp'), may hold values from 0 to 2, never falling along the last dimension, each value on 1 to 3072 neighbouring positions
- out_weight: bfloat16 [2048, 2048], P('tp'), may hold values from -0.125 to 0.125
- attn_gain: float32 [2048], replicated, may hold values from 0.1 to 1.9
- mlp_gain: float32 [2048], replicated, may hold values from 0.1 to 1.9
- gate_weight: bfloat16 [2048, 4096], P('sp', 'tp'), may hold values from -0.125 to 0.125
- up_weight: bfloat16 [2048, 4096], P('sp', 'tp'), may hold values from -0.125 to 0.125
- down_weight: bfloat16 [4096, 2048], P('tp', 'sp'), may hold values from -0.375 to 0.375
Outputs:
- mixed: bfloat16 [4096, 2048], P(('sp', 'tp'))
Inputs may be any that keep to these rules, and one draw needn't show every extreme that they name: `log_gates`: each head's row never rises from one position to the next and starts at or below 0. `documents`: document numbers never fall along the positions; one document spans exactly three quarters of the 4096 positions.
All inputs are finite; a program needn't handle non-finite values.
Results may differ from a plain program's by a relative error of at most 0.018.
Values may be sent and summed in bfloat16 or wider, within the bound.
A program may use at most 64 MiB of HBM per device.

v0:
```python
import math
import jax
import jax.numpy as jnp
from jax import lax
from jax.sharding import PartitionSpec as P

HD = 128


def local(
    resid,
    queries,
    keys,
    values,
    log_gates,
    documents,
    out_weight,
    attn_gain,
    mlp_gain,
    gate_weight,
    up_weight,
    down_weight,
):
    tok_rows = queries.shape[0]
    kv_dev = keys.shape[1] // HD
    heads_dev = log_gates.shape[0]
    group_size = heads_dev // kv_dev
    score_scale = 1.0 / math.sqrt(HD)
    own_start = lax.axis_index("sp") * tok_rows
    own_last = own_start + tok_rows - 1
    first_doc = documents[0]
    query_pos = own_start + lax.iota(jnp.int32, tok_rows)
    query_heads = queries.reshape(tok_rows, kv_dev, group_size, HD)
    key_gates_all = log_gates.reshape(kv_dev, group_size, log_gates.shape[1])
    query_gates = lax.dynamic_slice_in_dim(key_gates_all, own_start, tok_rows, 2)
    collected = (
        lax.all_gather(gate_weight, "sp", axis=0, tiled=True),
        lax.all_gather(up_weight, "sp", axis=0, tiled=True),
        lax.all_gather(down_weight, "sp", axis=1, tiled=True),
    )
    residual_rows = resid.astype(jnp.float32)

    def attend_block(running, key_rows, value_rows, doc_rows, first_row):
        run_max, run_sum, accumulated = running
        key_count = key_rows.shape[0]
        scores = (
            jnp.einsum(
                "tkgd,skd->kgts",
                query_heads,
                key_rows.reshape(key_count, kv_dev, HD),
                preferred_element_type=jnp.float32,
            )
            * score_scale
        )
        key_gates = lax.dynamic_slice_in_dim(key_gates_all, first_row, key_count, 2)
        scores = scores + query_gates[..., None] - key_gates[:, :, None, :]
        key_pos = first_row + lax.iota(jnp.int32, key_count)
        visible = (key_pos[None, :] <= query_pos[:, None]) & (
            doc_rows[None, :] == documents[:, None]
        )
        scores = jnp.where(visible, scores, jnp.float32(-1e30))
        new_max = jnp.maximum(run_max, jnp.max(scores, axis=-1))
        probs = jnp.where(visible, jnp.exp(scores - new_max[..., None]), jnp.float32(0.0))
        shrink = jnp.exp(run_max - new_max)
        run_sum = run_sum * shrink + jnp.sum(probs, axis=-1)
        weighted = jnp.einsum(
            "kgts,skd->kgtd",
            probs.astype(jnp.bfloat16),
            value_rows.reshape(key_count, kv_dev, HD),
            preferred_element_type=jnp.float32,
        )
        accumulated = accumulated * shrink[..., None] + weighted
        return (new_max, run_sum, accumulated)

    def maybe_attend(running, key_rows, value_rows, doc_rows, first_row):
        needed = (first_row <= own_last) & (doc_rows[-1] >= first_doc)

        def compute(state):
            return attend_block(state, key_rows, value_rows, doc_rows, first_row)

        def keep(state):
            return state

        return lax.cond(needed, compute, keep, running)

    start_state = (
        jnp.full((kv_dev, group_size, tok_rows), -1e30, jnp.float32),
        jnp.zeros((kv_dev, group_size, tok_rows), jnp.float32),
        jnp.zeros((kv_dev, group_size, tok_rows, HD), jnp.float32),
    )
    key_rows = lax.all_gather(keys, "sp", axis=0, tiled=True)
    value_rows = lax.all_gather(values, "sp", axis=0, tiled=True)
    doc_rows = lax.all_gather(documents, "sp", axis=0, tiled=True)
    key_count = key_rows.shape[0]
    block_len = math.gcd(key_count, 1024)

    def advance(block_index, inner):
        offset = block_index * block_len
        return maybe_attend(
            inner,
            lax.dynamic_slice_in_dim(key_rows, offset, block_len, 0),
            lax.dynamic_slice_in_dim(value_rows, offset, block_len, 0),
            lax.dynamic_slice_in_dim(doc_rows, offset, block_len, 0),
            offset,
        )

    run_max, run_sum, accumulated = lax.fori_loop(0, key_count // block_len, advance, start_state)
    attended = accumulated / run_sum[..., None]
    attended = (
        jnp.transpose(attended, (2, 0, 1, 3)).reshape(tok_rows, heads_dev * HD).astype(jnp.bfloat16)
    )
    rows_slice = attended
    projected = lax.psum_scatter(
        jnp.dot(rows_slice, out_weight, preferred_element_type=jnp.float32).astype(jnp.bfloat16),
        "tp",
        scatter_dimension=0,
        tiled=True,
    ).astype(jnp.float32)
    power = jnp.mean(projected * projected, axis=-1, keepdims=True)
    middle = residual_rows + attn_gain * projected * lax.rsqrt(power + 1e-06)
    middle_power = jnp.mean(middle * middle, axis=-1, keepdims=True)
    normed = (mlp_gain * middle * lax.rsqrt(middle_power + 1e-06)).astype(jnp.bfloat16)
    normed_all = lax.all_gather(normed, "tp", axis=0, tiled=True)
    gate_full, up_full, down_full = collected
    gate_act = jnp.dot(normed_all, gate_full, preferred_element_type=jnp.float32)
    up_act = jnp.dot(normed_all, up_full, preferred_element_type=jnp.float32)
    hidden = (jax.nn.silu(gate_act) * up_act).astype(jnp.bfloat16)
    rows_slice = hidden
    lowered = lax.psum_scatter(
        jnp.dot(rows_slice, down_full, preferred_element_type=jnp.float32).astype(jnp.bfloat16),
        "tp",
        scatter_dimension=0,
        tiled=True,
    ).astype(jnp.float32)
    return (middle + 0.5 * lowered).astype(jnp.bfloat16)


def solution(mesh):
    placed = (
        P(("sp", "tp"), None),
        P("sp", "tp"),
        P("sp", "tp"),
        P("sp", "tp"),
        P("tp", None),
        P("sp"),
        P("tp", None),
        P(),
        P(),
        P("sp", "tp"),
        P("sp", "tp"),
        P("tp", "sp"),
    )
    return jax.shard_map(
        local, mesh=mesh, in_specs=placed, out_specs=P(("sp", "tp"), None), check_vma=False
    )
```

profile of v0, /device:TPU:0, one launch (start us, length us, event | category | flops | bytes accessed | tf_op | source)
XLA Modules:
  0.0 661.0 jit_solution(3229841452047718858)
XLA Ops:
  6.5 0.0 all-gather.10.cloned.1.call-start
  6.5 1.8 copy.27
  8.3 0.0 all-gather.10.cloned.1.call-update
  8.4 0.0 all-gather.8.cloned.1.call-start
  8.4 1.8 copy.25
  10.2 0.0 all-gather.8.cloned.1.call-update
  10.2 0.0 reduce-scatter.3.cloned.1.call-start
  10.3 1.0 reshape.49
  11.3 1.2 copy.26
  12.5 0.3 copy.28
  12.8 1.2 slice.10
  14.0 43.0 %all-gather = s32[16,1,256]{2,1,0:T(1,128)S(1)} all-gather(s32[1,1,256]{2,1,0:T(1,128)} %bitcast.62), channel_id=1, replica_groups=mesh['sp'=16,'tp'=2] {'sp'}, dimensions={0}, use_global_device_ids=true | all-gather | bytes 17408 | tf_op jit(solution)/shard_map/all_gather | solution.py:93
  56.9 42.7 %all-gather.10.cloned.1.call-done = bf16[4096,512]{0,1:T(8,128)(2,1)} async-done(((bf16[256,512]{0,1:T(8,128)(2,1)}), bf16[4096,512]{0,1:T(8,128)(2,1)}) %all-gather.10.cloned.1.call-update) | async-done | bytes 4194320 | tf_op jit(solution)/shard_map/all_gather | solution.py:92
  99.7 87.7 %all-gather.8.cloned.1.call-done = bf16[4096,512]{0,1:T(8,128)(2,1)} async-done(((bf16[256,512]{0,1:T(8,128)(2,1)}), bf16[4096,512]{0,1:T(8,128)(2,1)}) %all-gather.8.cloned.1.call-update) | async-done | bytes 4194320 | tf_op jit(solution)/shard_map/all_gather | solution.py:91
  187.4 0.1 broadcast_in_dim.42
  187.5 20.5 %while.18 = (s32[]{:T(128)}, f32[4,2,256]{2,1,0:T(2,128)S(1)}, f32[4,2,256]{2,1,0:T(2,128)S(1)}, f32[4,2,256,128]{3,2,1,0:T(8,128)S(1)}, s32[]{:T(128)}, /*index...) while((s32[]{:T(128)}, f32[4,2,256]{2,1,0:T(2,128)S(1)}, ...), condition=%wide.region_5.6_spmd.clone, body=%wide.region_0.5_spmd.clone.sunk | while | flops 1114903808 | bytes 35472848 | solution.py:107
  187.5 0.6 slice.13
  189.3 13.1 %conditional.3 = ((f32[4,2,256]{2,1,0:T(2,128)S(1)}, f32[4,2,256]{2,1,0:T(2,128)S(1)}, f32[4,2,256,128]{3,2,1,0:T(8,128)S(1)})) conditional(s32[]{:T(128)} %convert_element_type.92, (f32[4,2,256]{2,1,0:T(2,128)S(1)}, f32[4,2,256]{2,1,0:T(2,128)S(1)}, f32[4,2,256,128]{3,2,1,0:T(8,128)S(1)}) %tuple.52, (s32[]{:T(128)}, s32[]{:T(128)}, ...), branch_computations={%region_1.0_spmd, %region_2.4_spmd} | conditional | flops 1114903808 | bytes 35463248 | solution.py:84
  189.4 1.0 compare_and_fusion
  190.4 1.7 constant_dynamic-slice_fusion
  192.2 3.0 fusion.6
  195.2 3.0 fusion.5
  198.3 4.1 fusion.10
  202.5 0.6 slice.13
  204.3 0.6 slice.13
  206.2 0.6 slice.13
  208.0 0.0 copy-start.1
  208.0 0.0 copy-start.2
  208.1 0.0 copy-start.3
  208.1 0.3 copy.29
  208.4 0.1 divide_convert_fusion
  208.5 4.4 convolution_convert_fusion
  213.0 0.0 reduce-scatter.3.cloned.1.call-update
  213.0 0.0 all-gather.12.cloned.1.call-start
  213.0 32.8 %reduce-scatter.3.cloned.1.call-done = bf16[128,2048]{1,0:T(8,128)(2,1)} async-done(((bf16[256,2048]{1,0:T(8,128)(2,1)}), bf16[128,2048]{1,0:T(8,128)(2,1)}) %reduce-scatter.3.cloned.1.call-update) | async-done | bytes 524304 | tf_op jit(solution)/shard_map/reduce_scatter | solution.py:113
  245.8 1.2 fusion.19
  247.1 0.0 copy-done.1
  247.1 0.0 copy-done.2
  247.1 1.4 multiply_reduce_fusion
  248.5 0.0 copy-done.3
  248.5 2.2 multiply_convert_fusion
  250.7 0.0 all-gather.12.cloned.1.call-update
  250.8 0.0 all-gather.14.cloned.1.call-start
  250.8 0.5 all-gather.14.cloned.1.call-update
  251.4 0.0 all-gather.16.cloned.1.call-start
  251.4 0.5 all-gather.16.cloned.1.call-update
  251.9 0.0 all-gather.18.cloned.1.call-start
  252.0 0.7 all-gather.18.cloned.1.call-update
  252.7 0.2 reduce-scatter.5.cloned.1.call-start
  252.9 8.2 %all-gather.12.cloned.1.call-done = bf16[256,2048]{1,0:T(8,128)(2,1)} async-done(((bf16[128,2048]{1,0:T(8,128)(2,1)}), bf16[256,2048]{1,0:T(8,128)(2,1)}) %all-gather.12.cloned.1.call-update) | async-done | bytes 1048592 | tf_op jit(solution)/shard_map/all_gather | solution.py:123
  261.2 0.0 copy-start.4
  261.2 116.1 %all-gather.14.cloned.1.call-done = bf16[2048,2048]{1,0:T(8,128)(2,1)} async-done(((bf16[128,2048]{1,0:T(8,128)(2,1)}), bf16[2048,2048]{1,0:T(8,128)(2,1)}) %all-gather.14.cloned.1.call-update) | async-done | bytes 8388624 | tf_op jit(solution)/shard_map/all_gather | solution.py:37
  377.3 7.4 %fusion.21 = f32[256,2048]{1,0:T(8,128)} fusion(bf16[256,2048]{1,0:T(8,128)(2,1)} %all-gather.12.cloned.1.call-done, bf16[2048,2048]{1,0:T(8,128)(2,1)} %all-gather.14.cloned.1.call-done), kind=kOutput, calls=%fused_computation.39 | convolution fusion | flops 2147483648 | bytes 11534336 | tf_op jit(solution)/shard_map/dot_general | solution.py:125
  384.7 0.0 copy-start
  384.7 105.7 %all-gather.16.cloned.1.call-done = bf16[2048,2048]{1,0:T(8,128)(2,1)} async-done(((bf16[128,2048]{1,0:T(8,128)(2,1)}), bf16[2048,2048]{1,0:T(8,128)(2,1)}) %all-gather.16.cloned.1.call-update) | async-done | bytes 8388624 | tf_op jit(solution)/shard_map/all_gather | solution.py:38
  490.4 142.7 %all-gather.18.cloned.1.call-done = bf16[2048,2048]{1,0:T(8,128)(2,1)} async-done(((bf16[2048,128]{1,0:T(8,128)(2,1)}), bf16[2048,2048]{1,0:T(8,128)(2,1)}) %all-gather.18.cloned.1.call-update) | async-done | bytes 8388624 | tf_op jit(solution)/shard_map/all_gather | solution.py:39
  633.1 0.0 copy-done.4
  633.1 12.1 %convolution_convert_fusion.1 = bf16[256,2048]{1,0:T(8,128)(2,1)} fusion(bf16[2048,2048]{1,0:T(8,128)(2,1)} %all-gather.18.cloned.1.call-done, bf16[256,2048]{1,0:T(8,128)(2,1)S(1)} %copy-done.4, bf16[2048,2048]{1,0:T(8,128)(2,1)} %all-gather.16.cloned.1.call-done, f32[256,2048]{1,0:T(8,128)} %fusion.21), kind=kOutput, calls=%fused_computation.25 | convolution fusion | flops 4298637312 | bytes 20971520 | tf_op jit(solution)/shard_map/dot_general | solution.py:130
  645.3 0.0 reduce-scatter.5.cloned.1.call-update
  645.3 6.7 %reduce-scatter.5.cloned.1.call-done = bf16[128,2048]{1,0:T(8,128)(2,1)} async-done(((bf16[256,2048]{1,0:T(8,128)(2,1)}), bf16[128,2048]{1,0:T(8,128)(2,1)}) %reduce-scatter.5.cloned.1.call-update) | async-done | bytes 524304 | tf_op jit(solution)/shard_map/reduce_scatter | solution.py:129
  652.0 0.0 copy-done
  652.0 2.2 add_convert_fusion
  (22 shorter events, 0.2 us)
Async XLA Ops:
  6.5 93.2 %all-gather.10.cloned.1.call-start = ((), (), s32[]{:S(2)}) async-start(), calls=%async_computation.3 | async-start | bytes 4456448 | tf_op jit(solution)/shard_map/all_gather | solution.py:92
  8.4 179.0 %all-gather.8.cloned.1.call-start = ((), (), s32[]{:S(2)}) async-start(), calls=%async_computation.2 | async-start | bytes 4456448 | tf_op jit(solution)/shard_map/all_gather | solution.py:91
  10.2 235.6 %reduce-scatter.3.cloned.1.call-start = ((), (), s32[]{:S(2)}) async-start(), calls=%async_computation.4 | async-start | bytes 1572864 | tf_op jit(solution)/shard_map/reduce_scatter | solution.py:113
  208.0 39.0 %copy-start.1 = (bf16[128,2048]{1,0:T(8,128)(2,1)S(1)}, bf16[128,2048]{1,0:T(8,128)(2,1)}, u32[]{:S(2)}) copy-start(bf16[128,2048]{1,0:T(8,128)(2,1)} %param.16) | copy-start | bytes 1572868
  208.0 39.0 %copy-start.2 = (f32[2048]{0:T(1024)S(1)}, f32[2048]{0:T(1024)}, u32[]{:S(2)}) copy-start(f32[2048]{0:T(1024)} %param.23) | copy-start | bytes 24580
  208.1 40.5 %copy-start.3 = (f32[2048]{0:T(1024)S(1)}, f32[2048]{0:T(1024)}, u32[]{:S(2)}) copy-start(f32[2048]{0:T(1024)} %param.24) | copy-start | bytes 24580
  213.0 48.2 %all-gather.12.cloned.1.call-start = ((), (), s32[]{:S(2)}) async-start(), calls=%async_computation.5 | async-start | bytes 1572864 | tf_op jit(solution)/shard_map/all_gather | solution.py:123
  250.8 126.5 %all-gather.14.cloned.1.call-start = ((), (), s32[]{:S(2)}) async-start(), calls=%async_computation.6 | async-start | bytes 8912896 | tf_op jit(solution)/shard_map/all_gather | solution.py:37
  251.4 239.1 %all-gather.16.cloned.1.call-start = ((), (), s32[]{:S(2)}) async-start(), calls=%async_computation.7 | async-start | bytes 8912896 | tf_op jit(solution)/shard_map/all_gather | solution.py:38
  251.9 381.2 %all-gather.18.cloned.1.call-start = ((), (), s32[]{:S(2)}) async-start(), calls=%async_computation.8 | async-start | bytes 8912896 | tf_op jit(solution)/shard_map/all_gather | solution.py:39
  252.7 399.4 %reduce-scatter.5.cloned.1.call-start = ((), (), s32[]{:S(2)}) async-start(), calls=%async_computation.9 | async-start | bytes 1572864 | tf_op jit(solution)/shard_map/reduce_scatter | solution.py:129
  261.2 372.0 %copy-start.4 = (bf16[256,2048]{1,0:T(8,128)(2,1)S(1)}, bf16[256,2048]{1,0:T(8,128)(2,1)}, u32[]{:S(2)}) copy-start(bf16[256,2048]{1,0:T(8,128)(2,1)} %all-gather.12.cloned.1.call-done) | copy-start | bytes 3145732
  384.7 267.3 %copy-start = (bf16[128,2048]{1,0:T(8,128)(2,1)S(1)}, bf16[128,2048]{1,0:T(8,128)(2,1)}, u32[]{:S(2)}) copy-start(bf16[128,2048]{1,0:T(8,128)(2,1)} %reduce-scatter.3.cloned.1.call-done) | copy-start | bytes 1572868
Sparse Core Ops, SparseCore 0:
  10.1 89.5 all-gather.9
  102.4 84.9 all-gather.7
  213.1 32.6 reduce-scatter.2
  250.9 10.2 all-gather.11
  263.8 113.4 all-gather.13
  379.9 110.4 all-gather.15
  493.1 139.9 all-gather.17
  645.4 6.5 reduce-scatter.4
where the time goes:
time: 662 us; the launch traced here: 661 us
  waiting for transfers between devices  545 us (82%)
  blocking collectives  43 us (6%)
  matrix products  31.2 us (5%)
  between operations  13.6 us (2%)
  local copies, waits for them, and re-layouts  11.9 us (2%)
  other arithmetic  11.2 us (2%)
    all_gather x1, waiting for transfers between devices, local(): lax.all_gather(down_weight, 'sp', axis=1, tiled=True)  143 us
    all_gather x1, waiting for transfers between devices, local(): lax.all_gather(gate_weight, 'sp', axis=0, tiled=True)  116 us
    all_gather x1, waiting for transfers between devices, local(): lax.all_gather(up_weight, 'sp', axis=0, tiled=True)  106 us
    all_gather x1, waiting for transfers between devices, local(): key_rows = lax.all_gather(keys, 'sp', axis=0, tiled=True)  87.7 us
    all_gather x1, blocking collectives, local(): doc_rows = lax.all_gather(documents, 'sp', axis=0, tiled=True)  43 us
    all_gather x1, waiting for transfers between devices, local(): value_rows = lax.all_gather(values, 'sp', axis=0, tiled=True)  42.7 us
    reduce_scatter x1, waiting for transfers between devices, local(): lax.psum_scatter(jnp.dot(rows_slice, out_weight, preferred_element_type=j...  32.8 us
  transfers between devices with their start and end apart: 8, of which 8 were waited for; matrix products, arithmetic and copies ran while one was open for 2% of the time, Pallas kernels for 0%

commit v1 on v0

--- a/solution.py
+++ b/solution.py
@@ -88,7 +88,22 @@
         jnp.zeros((kv_dev, group_size, tok_rows), jnp.float32),
         jnp.zeros((kv_dev, group_size, tok_rows, HD), jnp.float32),
     )
-    key_rows = lax.all_gather(keys, "sp", axis=0, tiled=True)
+
+    def goods_serve(mesh_ax, my_tile):
+        axis_total = jax.lax.axis_size(mesh_ax)
+        piece_next = [(idx - 1, idx) for idx in range(1, axis_total)] + [(axis_total - 1, 0)]
+        n_now = my_tile
+        inbox = [n_now]
+        for _ in range(axis_total - 1):
+            n_now = jax.lax.ppermute(n_now, axis_name=mesh_ax, perm=piece_next)
+            inbox += [n_now]
+        return jnp.roll(
+            jnp.concatenate([*reversed(inbox)], axis=0),
+            shift=(jax.lax.axis_index(mesh_ax) + 1) * n_now.shape[0],
+            axis=0,
+        )
+
+    key_rows = goods_serve("sp", keys)
     value_rows = lax.all_gather(values, "sp", axis=0, tiled=True)
     doc_rows = lax.all_gather(documents, "sp", axis=0, tiled=True)
     key_count = key_rows.shape[0]

time: 662 us -> 716 us (1.082)
  waiting for transfers between devices: 545 us -> 579 us
  local copies, waits for them, and re-layouts: 11.9 us -> 26.9 us
    ppermute x0 -> x15, waiting for transfers between devices: none -> 173 us  [goods_serve(): n_now = jax.lax.ppermute(n_now, axis_name=mesh_ax, perm=piece_next)]
    all_gather x1 -> x0, waiting for transfers between devices: 87.7 us -> none  [local(): key_rows = lax.all_gather(keys, 'sp', axis=0, tiled=True)]
    all_gather x1, waiting for transfers between devices: 42.7 us -> 0.01 us  [local(): value_rows = lax.all_gather(values, 'sp', axis=0, tiled=True)]
    unnamed x14 -> x59, local copies, waits for them, and re-layouts: 5.14 us -> 14.8 us
    reduce_scatter x1, waiting for transfers between devices: 32.8 us -> 24.9 us  [local(): lax.psum_scatter(jnp.dot(rows_slice, out_weight, preferred_element_type=j...]
  transfers between devices with their start and end apart: 8 -> 22, of which waited for: 8 -> 20; matrix products, arithmetic and copies ran while one was open for 2% -> 3% of each run, Pallas kernels for 0% -> 0%
where the time goes in v1:
time: 716 us; the launch traced here: 715 us
  waiting for transfers between devices  579 us (81%)
  blocking collectives  43.2 us (6%)
  matrix products  32.2 us (4%)
  local copies, waits for them, and re-layouts  26.9 us (4%)
  between operations  13.9 us (2%)
  other arithmetic  10.6 us (1%)
    ppermute x15, waiting for transfers between devices, goods_serve(): n_now = jax.lax.ppermute(n_now, axis_name=mesh_ax, perm=piece_next)  173 us
    all_gather x1, waiting for transfers between devices, local(): lax.all_gather(down_weight, 'sp', axis=1, tiled=True)  143 us
    all_gather x1, waiting for transfers between devices, local(): lax.all_gather(gate_weight, 'sp', axis=0, tiled=True)  116 us
    all_gather x1, waiting for transfers between devices, local(): lax.all_gather(up_weight, 'sp', axis=0, tiled=True)  106 us
    all_gather x1, blocking collectives, local(): doc_rows = lax.all_gather(documents, 'sp', axis=0, tiled=True)  43.2 us
    reduce_scatter x1, waiting for transfers between devices, local(): lax.psum_scatter(jnp.dot(rows_slice, out_weight, preferred_element_type=j...  24.9 us
    unnamed x59, local copies, waits for them, and re-layouts  14.8 us
  transfers between devices with their start and end apart: 22, of which 20 were waited for; matrix products, arithmetic and copies ran while one was open for 3% of the time, Pallas kernels for 0%

profile of v1, /device:TPU:0, one launch (start us, length us, event | category | flops | bytes accessed | tf_op | source)
XLA Modules:
  0.0 715.0 jit_solution(18133810573093827618)
XLA Ops:
  6.5 1.1 copy.27
  7.6 3.0 collective-permute-start
  10.6 10.3 %collective-permute-done = bf16[256,512]{0,1:T(8,128)(2,1)S(1)} collective-permute-done((bf16[256,512]{0,1:T(8,128)(2,1)S(1)}, bf16[256,512]{0,1:T(8,128)(2,1)S(1)}, u32[]{:S(2)}, u32[]{:S(2)}) %collective-permute-start) | collective-permute-done | bytes 262176 | tf_op jit(solution)/shard_map/ppermute | solution.py:98
  20.9 1.8 copy.31
  22.8 9.2 %collective-permute-done.1 = bf16[256,512]{0,1:T(8,128)(2,1)S(1)} collective-permute-done((bf16[256,512]{0,1:T(8,128)(2,1)S(1)}, bf16[256,512]{0,1:T(8,128)(2,1)S(1)}, u32[]{:S(2)}, u32[]{:S(2)}) %collective-permute-start.1) | collective-permute-done | bytes 262176 | tf_op jit(solution)/shard_map/ppermute | solution.py:98
  32.0 11.8 %collective-permute-done.2 = bf16[256,512]{0,1:T(8,128)(2,1)S(1)} collective-permute-done((bf16[256,512]{0,1:T(8,128)(2,1)S(1)}, bf16[256,512]{0,1:T(8,128)(2,1)S(1)}, u32[]{:S(2)}, u32[]{:S(2)}) %collective-permute-start.2) | collective-permute-done | bytes 262176 | tf_op jit(solution)/shard_map/ppermute | solution.py:98
  43.8 10.0 %collective-permute-done.3 = bf16[256,512]{0,1:T(8,128)(2,1)S(1)} collective-permute-done((bf16[256,512]{0,1:T(8,128)(2,1)S(1)}, bf16[256,512]{0,1:T(8,128)(2,1)S(1)}, u32[]{:S(2)}, u32[]{:S(2)}) %collective-permute-start.3) | collective-permute-done | bytes 262176 | tf_op jit(solution)/shard_map/ppermute | solution.py:98
  53.8 14.1 %collective-permute-done.4 = bf16[256,512]{0,1:T(8,128)(2,1)S(1)} collective-permute-done((bf16[256,512]{0,1:T(8,128)(2,1)S(1)}, bf16[256,512]{0,1:T(8,128)(2,1)S(1)}, u32[]{:S(2)}, u32[]{:S(2)}) %collective-permute-start.4) | collective-permute-done | bytes 262176 | tf_op jit(solution)/shard_map/ppermute | solution.py:98
  67.9 14.1 %collective-permute-done.5 = bf16[256,512]{0,1:T(8,128)(2,1)S(1)} collective-permute-done((bf16[256,512]{0,1:T(8,128)(2,1)S(1)}, bf16[256,512]{0,1:T(8,128)(2,1)S(1)}, u32[]{:S(2)}, u32[]{:S(2)}) %collective-permute-start.5) | collective-permute-done | bytes 262176 | tf_op jit(solution)/shard_map/ppermute | solution.py:98
  82.0 18.1 %collective-permute-done.6 = bf16[256,512]{0,1:T(8,128)(2,1)S(1)} collective-permute-done((bf16[256,512]{0,1:T(8,128)(2,1)S(1)}, bf16[256,512]{0,1:T(8,128)(2,1)S(1)}, u32[]{:S(2)}, u32[]{:S(2)}) %collective-permute-start.6) | collective-permute-done | bytes 262176 | tf_op jit(solution)/shard_map/ppermute | solution.py:98
  100.1 18.0 %collective-permute-done.7 = bf16[256,512]{0,1:T(8,128)(2,1)S(1)} collective-permute-done((bf16[256,512]{0,1:T(8,128)(2,1)S(1)}, bf16[256,512]{0,1:T(8,128)(2,1)S(1)}, u32[]{:S(2)}, u32[]{:S(2)}) %collective-permute-start.7) | collective-permute-done | bytes 262176 | tf_op jit(solution)/shard_map/ppermute | solution.py:98
  118.1 17.7 %collective-permute-done.8 = bf16[256,512]{0,1:T(8,128)(2,1)S(1)} collective-permute-done((bf16[256,512]{0,1:T(8,128)(2,1)S(1)}, bf16[256,512]{0,1:T(8,128)(2,1)S(1)}, u32[]{:S(2)}, u32[]{:S(2)}) %collective-permute-start.8) | collective-permute-done | bytes 262176 | tf_op jit(solution)/shard_map/ppermute | solution.py:98
  135.8 10.0 %collective-permute-done.9 = bf16[256,512]{0,1:T(8,128)(2,1)S(1)} collective-permute-done((bf16[256,512]{0,1:T(8,128)(2,1)S(1)}, bf16[256,512]{0,1:T(8,128)(2,1)S(1)}, u32[]{:S(2)}, u32[]{:S(2)}) %collective-permute-start.9) | collective-permute-done | bytes 262176 | tf_op jit(solution)/shard_map/ppermute | solution.py:98
  145.7 10.0 %collective-permute-done.10 = bf16[256,512]{0,1:T(8,128)(2,1)S(1)} collective-permute-done((bf16[256,512]{0,1:T(8,128)(2,1)S(1)}, bf16[256,512]{0,1:T(8,128)(2,1)S(1)}, u32[]{:S(2)}, u32[]{:S(2)}) %collective-permute-start.10) | collective-permute-done | bytes 262176 | tf_op jit(solution)/shard_map/ppermute | solution.py:98
  155.7 0.7 copy-done.2
  156.4 10.0 %collective-permute-done.11 = bf16[256,512]{0,1:T(8,128)(2,1)S(1)} collective-permute-done((bf16[256,512]{0,1:T(8,128)(2,1)S(1)}, bf16[256,512]{0,1:T(8,128)(2,1)S(1)}, u32[]{:S(2)}, u32[]{:S(2)}) %collective-permute-start.11) | collective-permute-done | bytes 262176 | tf_op jit(solution)/shard_map/ppermute | solution.py:98
  166.4 0.7 copy-done.4
  167.1 10.0 %collective-permute-done.12 = bf16[256,512]{0,1:T(8,128)(2,1)S(1)} collective-permute-done((bf16[256,512]{0,1:T(8,128)(2,1)S(1)}, bf16[256,512]{0,1:T(8,128)(2,1)S(1)}, u32[]{:S(2)}, u32[]{:S(2)}) %collective-permute-start.12) | collective-permute-done | bytes 262176 | tf_op jit(solution)/shard_map/ppermute | solution.py:98
  177.1 0.7 copy-done.6
  177.8 10.1 %collective-permute-done.13 = bf16[256,512]{0,1:T(8,128)(2,1)} collective-permute-done((bf16[256,512]{0,1:T(8,128)(2,1)S(1)}, bf16[256,512]{0,1:T(8,128)(2,1)}, u32[]{:S(2)}, u32[]{:S(2)}) %collective-permute-start.13) | collective-permute-done | bytes 262176 | tf_op jit(solution)/shard_map/ppermute | solution.py:98
  187.9 1.0 reshape.49
  188.8 1.2 copy.30
  190.1 1.0 copy.32
  191.1 1.3 slice.10
  192.4 43.2 %all-gather = s32[16,1,256]{2,1,0:T(1,128)} all-gather(s32[1,1,256]{2,1,0:T(1,128)} %bitcast.62), channel_id=1, replica_groups=mesh['sp'=16,'tp'=2] {'sp'}, dimensions={0}, use_global_device_ids=true | all-gather | bytes 17408 | tf_op jit(solution)/shard_map/all_gather | solution.py:108
  235.6 1.0 constant_dynamic-update-slice_fusion.31
  236.6 1.0 constant_dynamic-update-slice_fusion.30
  237.6 1.0 constant_dynamic-update-slice_fusion.29
  238.5 1.0 constant_dynamic-update-slice_fusion.28
  239.5 1.0 constant_dynamic-update-slice_fusion.27
  240.9 1.0 constant_dynamic-update-slice_fusion.15
  241.9 1.0 constant_dynamic-update-slice_fusion.14
  243.4 2.3 constant_dynamic-slice_fusion.4
  245.8 24.2 %while.18 = (s32[]{:T(128)}, f32[4,2,256]{2,1,0:T(2,128)S(1)}, f32[4,2,256]{2,1,0:T(2,128)S(1)}, f32[4,2,256,128]{3,2,1,0:T(8,128)S(1)}, s32[]{:T(128)}, /*index...) while((s32[]{:T(128)}, f32[4,2,256]{2,1,0:T(2,128)S(1)}, ...), condition=%wide.region_5.6_spmd.clone, body=%wide.region_0.5_spmd.clone.sunk | while | flops 1114903808 | bytes 35472848 | solution.py:122
  245.9 0.7 dynamic_slice.52
  246.6 0.7 slice.13
  248.5 13.4 %conditional.3 = ((f32[4,2,256]{2,1,0:T(2,128)S(1)}, f32[4,2,256]{2,1,0:T(2,128)S(1)}, f32[4,2,256,128]{3,2,1,0:T(8,128)S(1)})) conditional(s32[]{:T(128)} %convert_element_type.92, (f32[4,2,256]{2,1,0:T(2,128)S(1)}, f32[4,2,256]{2,1,0:T(2,128)S(1)}, f32[4,2,256,128]{3,2,1,0:T(8,128)S(1)}) %tuple.52, (s32[]{:T(128)}, s32[]{:T(128)}, ...), branch_computations={%region_1.1_spmd, %region_2.4_spmd} | conditional | flops 1114903808 | bytes 35463248 | solution.py:84
  248.6 0.3 compare_and_fusion
  248.9 1.7 constant_dynamic-slice_fusion
  250.7 4.1 fusion.6
  254.7 3.0 fusion.5
  257.8 4.1 fusion.10
  262.0 0.7 dynamic_slice.52
  262.7 0.7 slice.13
  264.7 0.7 dynamic_slice.52
  265.4 0.7 slice.13
  267.4 0.7 dynamic_slice.52
  268.1 0.7 slice.13
  270.6 4.4 convolution_convert_fusion
  275.1 24.9 %reduce-scatter.3.cloned.1.call-done = bf16[128,2048]{1,0:T(8,128)(2,1)} async-done(((bf16[256,2048]{1,0:T(8,128)(2,1)}), bf16[128,2048]{1,0:T(8,128)(2,1)}) %reduce-scatter.3.cloned.1.call-update) | async-done | bytes 524304 | tf_op jit(solution)/shard_map/reduce_scatter | solution.py:128
  299.9 1.2 fusion.19
  301.2 1.4 multiply_reduce_fusion
  302.6 2.2 multiply_convert_fusion
  304.9 0.5 all-gather.11.cloned.1.call-update
  305.5 0.5 all-gather.13.cloned.1.call-update
  306.1 0.5 all-gather.15.cloned.1.call-update
  306.9 8.4 %all-gather.9.cloned.1.call-done = bf16[256,2048]{1,0:T(8,128)(2,1)} async-done(((bf16[128,2048]{1,0:T(8,128)(2,1)}), bf16[256,2048]{1,0:T(8,128)(2,1)}) %all-gather.9.cloned.1.call-update) | async-done | bytes 1048592 | tf_op jit(solution)/shard_map/all_gather | solution.py:138
  315.3 116.1 %all-gather.11.cloned.1.call-done = bf16[2048,2048]{1,0:T(8,128)(2,1)} async-done(((bf16[128,2048]{1,0:T(8,128)(2,1)}), bf16[2048,2048]{1,0:T(8,128)(2,1)}) %all-gather.11.cloned.1.call-update) | async-done | bytes 8388624 | tf_op jit(solution)/shard_map/all_gather | solution.py:37
  431.4 7.4 %fusion.21 = f32[256,2048]{1,0:T(8,128)} fusion(bf16[256,2048]{1,0:T(8,128)(2,1)} %all-gather.9.cloned.1.call-done, bf16[2048,2048]{1,0:T(8,128)(2,1)} %all-gather.11.cloned.1.call-done), kind=kOutput, calls=%fused_computation.72 | convolution fusion | flops 2147483648 | bytes 11534336 | tf_op jit(solution)/shard_map/dot_general | solution.py:140
  438.8 105.7 %all-gather.13.cloned.1.call-done = bf16[2048,2048]{1,0:T(8,128)(2,1)} async-done(((bf16[128,2048]{1,0:T(8,128)(2,1)}), bf16[2048,2048]{1,0:T(8,128)(2,1)}) %all-gather.13.cloned.1.call-update) | async-done | bytes 8388624 | tf_op jit(solution)/shard_map/all_gather | solution.py:38
  544.5 142.6 %all-gather.15.cloned.1.call-done = bf16[2048,2048]{1,0:T(8,128)(2,1)} async-done(((bf16[2048,128]{1,0:T(8,128)(2,1)}), bf16[2048,2048]{1,0:T(8,128)(2,1)}) %all-gather.15.cloned.1.call-update) | async-done | bytes 8388624 | tf_op jit(solution)/shard_map/all_gather | solution.py:39
  687.1 12.1 %convolution_convert_fusion.1 = bf16[256,2048]{1,0:T(8,128)(2,1)} fusion(bf16[2048,2048]{1,0:T(8,128)(2,1)} %all-gather.15.cloned.1.call-done, bf16[256,2048]{1,0:T(8,128)(2,1)S(1)} %copy-done.11, bf16[2048,2048]{1,0:T(8,128)(2,1)} %all-gather.13.cloned.1.call-done, f32[256,2048]{1,0:T(8,128)} %fusion.21), kind=kOutput, calls=%fused_computation.25 | convolution fusion | flops 4298637312 | bytes 20971520 | tf_op jit(solution)/shard_map/dot_general | solution.py:145
  699.3 6.7 reduce-scatter.5.cloned.1.call-done
  706.0 2.2 add_convert_fusion
  (94 shorter events, 1.9 us)
Async XLA Ops:
  6.5 239.2 %all-gather.7.cloned.1.call-start = ((), (), s32[]{:S(2)}) async-start(), calls=%async_computation.2 | async-start | bytes 4456448 | tf_op jit(solution)/shard_map/all_gather | solution.py:107
  7.6 13.3 %collective-permute-start = (bf16[256,512]{0,1:T(8,128)(2,1)S(1)}, bf16[256,512]{0,1:T(8,128)(2,1)S(1)}, u32[]{:S(2)}, u32[]{:S(2)}) collective-permute-start(bf16[256,512]{0,1:T(8,128)(2,1)S(1)} %copy.27), channel_id=1, source_target_pairs={{0,2},{2,4},{4,6},{6,8},{8,10},{10,12},{12,14},{14,16},{16,18},{18... | collective-permute-start | bytes 786440 | tf_op jit(solution)/shard_map/ppermute | solution.py:98
  20.9 11.1 %collective-permute-start.1 = (bf16[256,512]{0,1:T(8,128)(2,1)S(1)}, bf16[256,512]{0,1:T(8,128)(2,1)S(1)}, u32[]{:S(2)}, u32[]{:S(2)}) collective-permute-start(bf16[256,512]{0,1:T(8,128)(2,1)S(1)} %collective-permute-done), channel_id=1, source_target_pairs={{0,2},{2,4},{4,6},{6,8},{8,10},{10,12},{12,14},{14,16},{16,18},{18... | collective-permute-start | bytes 786440 | tf_op jit(solution)/shard_map/ppermute | solution.py:98
  22.8 277.2 %reduce-scatter.3.cloned.1.call-start = ((), (), s32[]{:S(2)}) async-start(), calls=%async_computation.3 | async-start | bytes 1572864 | tf_op jit(solution)/shard_map/reduce_scatter | solution.py:128
  32.0 11.8 %collective-permute-start.2 = (bf16[256,512]{0,1:T(8,128)(2,1)S(1)}, bf16[256,512]{0,1:T(8,128)(2,1)S(1)}, u32[]{:S(2)}, u32[]{:S(2)}) collective-permute-start(bf16[256,512]{0,1:T(8,128)(2,1)S(1)} %collective-permute-done.1), channel_id=1, source_target_pairs={{0,2},{2,4},{4,6},{6,8},{8,10},{10,12},{12,14},{14,16},{16,18},{18... | collective-permute-start | bytes 786440 | tf_op jit(solution)/shard_map/ppermute | solution.py:98
  43.8 10.0 %collective-permute-start.3 = (bf16[256,512]{0,1:T(8,128)(2,1)S(1)}, bf16[256,512]{0,1:T(8,128)(2,1)S(1)}, u32[]{:S(2)}, u32[]{:S(2)}) collective-permute-start(bf16[256,512]{0,1:T(8,128)(2,1)S(1)} %collective-permute-done.2), channel_id=1, source_target_pairs={{0,2},{2,4},{4,6},{6,8},{8,10},{10,12},{12,14},{14,16},{16,18},{18... | collective-permute-start | bytes 786440 | tf_op jit(solution)/shard_map/ppermute | solution.py:98
  53.8 14.1 %collective-permute-start.4 = (bf16[256,512]{0,1:T(8,128)(2,1)S(1)}, bf16[256,512]{0,1:T(8,128)(2,1)S(1)}, u32[]{:S(2)}, u32[]{:S(2)}) collective-permute-start(bf16[256,512]{0,1:T(8,128)(2,1)S(1)} %collective-permute-done.3), channel_id=1, source_target_pairs={{0,2},{2,4},{4,6},{6,8},{8,10},{10,12},{12,14},{14,16},{16,18},{18... | collective-permute-start | bytes 786440 | tf_op jit(solution)/shard_map/ppermute | solution.py:98
  67.9 14.1 %collective-permute-start.5 = (bf16[256,512]{0,1:T(8,128)(2,1)S(1)}, bf16[256,512]{0,1:T(8,128)(2,1)S(1)}, u32[]{:S(2)}, u32[]{:S(2)}) collective-permute-start(bf16[256,512]{0,1:T(8,128)(2,1)S(1)} %collective-permute-done.4), channel_id=1, source_target_pairs={{0,2},{2,4},{4,6},{6,8},{8,10},{10,12},{12,14},{14,16},{16,18},{18... | collective-permute-start | bytes 786440 | tf_op jit(solution)/shard_map/ppermute | solution.py:98
  82.0 18.1 %collective-permute-start.6 = (bf16[256,512]{0,1:T(8,128)(2,1)S(1)}, bf16[256,512]{0,1:T(8,128)(2,1)S(1)}, u32[]{:S(2)}, u32[]{:S(2)}) collective-permute-start(bf16[256,512]{0,1:T(8,128)(2,1)S(1)} %collective-permute-done.5), channel_id=1, source_target_pairs={{0,2},{2,4},{4,6},{6,8},{8,10},{10,12},{12,14},{14,16},{16,18},{18... | collective-permute-start | bytes 786440 | tf_op jit(solution)/shard_map/ppermute | solution.py:98
  100.1 18.0 %collective-permute-start.7 = (bf16[256,512]{0,1:T(8,128)(2,1)S(1)}, bf16[256,512]{0,1:T(8,128)(2,1)S(1)}, u32[]{:S(2)}, u32[]{:S(2)}) collective-permute-start(bf16[256,512]{0,1:T(8,128)(2,1)S(1)} %collective-permute-done.6), channel_id=1, source_target_pairs={{0,2},{2,4},{4,6},{6,8},{8,10},{10,12},{12,14},{14,16},{16,18},{18... | collective-permute-start | bytes 786440 | tf_op jit(solution)/shard_map/ppermute | solution.py:98
  118.1 17.7 %collective-permute-start.8 = (bf16[256,512]{0,1:T(8,128)(2,1)S(1)}, bf16[256,512]{0,1:T(8,128)(2,1)S(1)}, u32[]{:S(2)}, u32[]{:S(2)}) collective-permute-start(bf16[256,512]{0,1:T(8,128)(2,1)S(1)} %collective-permute-done.7), channel_id=1, source_target_pairs={{0,2},{2,4},{4,6},{6,8},{8,10},{10,12},{12,14},{14,16},{16,18},{18... | collective-permute-start | bytes 786440 | tf_op jit(solution)/shard_map/ppermute | solution.py:98
  135.8 10.0 %collective-permute-start.9 = (bf16[256,512]{0,1:T(8,128)(2,1)S(1)}, bf16[256,512]{0,1:T(8,128)(2,1)S(1)}, u32[]{:S(2)}, u32[]{:S(2)}) collective-permute-start(bf16[256,512]{0,1:T(8,128)(2,1)S(1)} %collective-permute-done.8), channel_id=1, source_target_pairs={{0,2},{2,4},{4,6},{6,8},{8,10},{10,12},{12,14},{14,16},{16,18},{18... | collective-permute-start | bytes 786440 | tf_op jit(solution)/shard_map/ppermute | solution.py:98
  145.7 10.0 %collective-permute-start.10 = (bf16[256,512]{0,1:T(8,128)(2,1)S(1)}, bf16[256,512]{0,1:T(8,128)(2,1)S(1)}, u32[]{:S(2)}, u32[]{:S(2)}) collective-permute-start(bf16[256,512]{0,1:T(8,128)(2,1)S(1)} %collective-permute-done.9), channel_id=1, source_target_pairs={{0,2},{2,4},{4,6},{6,8},{8,10},{10,12},{12,14},{14,16},{16,18},{18... | collective-permute-start | bytes 786440 | tf_op jit(solution)/shard_map/ppermute | solution.py:98
  155.7 0.7 copy-start.2
  156.4 10.0 %collective-permute-start.11 = (bf16[256,512]{0,1:T(8,128)(2,1)S(1)}, bf16[256,512]{0,1:T(8,128)(2,1)S(1)}, u32[]{:S(2)}, u32[]{:S(2)}) collective-permute-start(bf16[256,512]{0,1:T(8,128)(2,1)S(1)} %collective-permute-done.10), channel_id=1, source_target_pairs={{0,2},{2,4},{4,6},{6,8},{8,10},{10,12},{12,14},{14,16},{16,18},{18... | collective-permute-start | bytes 786440 | tf_op jit(solution)/shard_map/ppermute | solution.py:98
  166.4 0.7 copy-start.4
  167.1 10.0 %collective-permute-start.12 = (bf16[256,512]{0,1:T(8,128)(2,1)S(1)}, bf16[256,512]{0,1:T(8,128)(2,1)S(1)}, u32[]{:S(2)}, u32[]{:S(2)}) collective-permute-start(bf16[256,512]{0,1:T(8,128)(2,1)S(1)} %collective-permute-done.11), channel_id=1, source_target_pairs={{0,2},{2,4},{4,6},{6,8},{8,10},{10,12},{12,14},{14,16},{16,18},{18... | collective-permute-start | bytes 786440 | tf_op jit(solution)/shard_map/ppermute | solution.py:98
  177.1 0.7 copy-start.6
  177.8 10.1 %collective-permute-start.13 = (bf16[256,512]{0,1:T(8,128)(2,1)S(1)}, bf16[256,512]{0,1:T(8,128)(2,1)}, u32[]{:S(2)}, u32[]{:S(2)}) collective-permute-start(bf16[256,512]{0,1:T(8,128)(2,1)S(1)} %collective-permute-done.12), channel_id=1, source_target_pairs={{0,2},{2,4},{4,6},{6,8},{8,10},{10,12},{12,14},{14,16},{16,18},{18... | collective-permute-start | bytes 786440 | tf_op jit(solution)/shard_map/ppermute | solution.py:98
  187.8 47.7 %collective-permute-start.14 = (bf16[256,512]{0,1:T(8,128)(2,1)}, bf16[256,512]{0,1:T(8,128)(2,1)}, u32[]{:S(2)}, u32[]{:S(2)}) collective-permute-start(bf16[256,512]{0,1:T(8,128)(2,1)} %collective-permute-done.13), channel_id=1, source_target_pairs={{0,2},{2,4},{4,6},{6,8},{8,10},{10,12},{12,14},{14,16},{16,18},{18... | collective-permute-start | bytes 786440 | tf_op jit(solution)/shard_map/ppermute | solution.py:98
  191.1 51.9 %copy-start.5 = (bf16[256,512]{0,1:T(8,128)(2,1)S(1)}, bf16[256,512]{0,1:T(8,128)(2,1)}, u32[]{:S(2)}) copy-start(bf16[256,512]{0,1:T(8,128)(2,1)} %copy-done.4) | copy-start | bytes 786436
  191.1 51.9 %copy-start.3 = (bf16[256,512]{0,1:T(8,128)(2,1)S(1)}, bf16[256,512]{0,1:T(8,128)(2,1)}, u32[]{:S(2)}) copy-start(bf16[256,512]{0,1:T(8,128)(2,1)} %copy-done.2) | copy-start | bytes 786436
  192.4 50.5 %copy-start.7 = (bf16[256,512]{0,1:T(8,128)(2,1)S(1)}, bf16[256,512]{0,1:T(8,128)(2,1)}, u32[]{:S(2)}) copy-start(bf16[256,512]{0,1:T(8,128)(2,1)} %copy-done.6) | copy-start | bytes 786436
  242.9 2.9 copy-start.9
  270.1 31.1 %copy-start.1 = (bf16[128,2048]{1,0:T(8,128)(2,1)S(1)}, bf16[128,2048]{1,0:T(8,128)(2,1)}, u32[]{:S(2)}) copy-start(bf16[128,2048]{1,0:T(8,128)(2,1)} %param.16) | copy-start | bytes 1572868
  270.1 31.1 %copy-start.8 = (f32[2048]{0:T(1024)S(1)}, f32[2048]{0:T(1024)}, u32[]{:S(2)}) copy-start(f32[2048]{0:T(1024)} %param.23) | copy-start | bytes 24580
  270.1 32.5 %copy-start.10 = (f32[2048]{0:T(1024)S(1)}, f32[2048]{0:T(1024)}, u32[]{:S(2)}) copy-start(f32[2048]{0:T(1024)} %param.24) | copy-start | bytes 24580
  275.0 40.2 %all-gather.9.cloned.1.call-start = ((), (), s32[]{:S(2)}) async-start(), calls=%async_computation.4 | async-start | bytes 1572864 | tf_op jit(solution)/shard_map/all_gather | solution.py:138
  304.9 126.5 %all-gather.11.cloned.1.call-start = ((), (), s32[]{:S(2)}) async-start(), calls=%async_computation.5 | async-start | bytes 8912896 | tf_op jit(solution)/shard_map/all_gather | solution.py:37
  305.4 239.1 %all-gather.13.cloned.1.call-start = ((), (), s32[]{:S(2)}) async-start(), calls=%async_computation.6 | async-start | bytes 8912896 | tf_op jit(solution)/shard_map/all_gather | solution.py:38
  306.0 381.1 %all-gather.15.cloned.1.call-start = ((), (), s32[]{:S(2)}) async-start(), calls=%async_computation.7 | async-start | bytes 8912896 | tf_op jit(solution)/shard_map/all_gather | solution.py:39
  306.6 399.4 %reduce-scatter.5.cloned.1.call-start = ((), (), s32[]{:S(2)}) async-start(), calls=%async_computation.8 | async-start | bytes 1572864 | tf_op jit(solution)/shard_map/reduce_scatter | solution.py:144
  315.3 371.8 %copy-start.11 = (bf16[256,2048]{1,0:T(8,128)(2,1)S(1)}, bf16[256,2048]{1,0:T(8,128)(2,1)}, u32[]{:S(2)}) copy-start(bf16[256,2048]{1,0:T(8,128)(2,1)} %all-gather.9.cloned.1.call-done) | copy-start | bytes 3145732
  438.8 267.2 %copy-start = (bf16[128,2048]{1,0:T(8,128)(2,1)S(1)}, bf16[128,2048]{1,0:T(8,128)(2,1)}, u32[]{:S(2)}) copy-start(bf16[128,2048]{1,0:T(8,128)(2,1)} %reduce-scatter.3.cloned.1.call-done) | copy-start | bytes 1572868
Sparse Core Ops, SparseCore 0:
  22.9 97.2 all-gather.6
  275.2 24.7 reduce-scatter.2
  305.0 10.2 all-gather.8
  317.9 113.4 all-gather.10
  434.0 110.4 all-gather.12
  547.1 139.9 all-gather.14
  699.4 6.5 reduce-scatter.4
